TPU v7x, 32 devices: a whole 2x2x4 slice. The times are simulated.
32 devices in a mesh: sp: 16 (over z, y, x), tp: 2 (over core).
Axes of the slice: x: 2, y: 2, z: 4, core: 2. Of those that a mesh axis runs over, the one named last changes fastest.
Arguments:
- resid: bfloat16 [8192, 2048], P('sp'), may hold values from -6 to 6
- queries: bfloat16 [8192, 2048], P('sp', 'tp'), may hold values from -6 to 6
- keys: bfloat16 [8192, 512], P('sp', 'tp'), may hold values from -6 to 6
- values: bfloat16 [8192, 512], P('sp', 'tp'), may hold values from -6 to 6
- documents: int32 [8192], P('sp'), may hold values from 0 to 7, never falling along the last dimension, each value on 1 to 2048 neighbouring positions
- q_gain: float32 [64], replicated, may hold values from 0.5 to 6.5
- k_gain: float32 [64], replicated, may hold values from 0.5 to 6.5
- sink: float32 [32], P('tp'), may hold values from -1 to 5
- w_out: bfloat16 [2048, 2048], P('tp'), may hold values from -0.5 to 0.5
- n_gain: float32 [2048], replicated, may hold values from 0.1 to 1.9
- w_up: bfloat16 [2048, 8192], P('sp', 'tp'), may hold values from -0.125 to 0.125
- w_down: bfloat16 [8192, 2048], P('tp', 'sp'), may hold values from -0.0625 to 0.0625
Outputs:
- layer_out: bfloat16 [8192, 2048], P('sp')
All inputs are finite; a program needn't handle non-finite values.
Results may differ from a plain program's by a relative error of at most 0.018.
The roundings to bfloat16 on the way count: a program that leaves them out, or rounds other values in their place, can miss the bound.
Values may be sent and summed in bfloat16 or wider, within the bound.
A program may use at most 128 MiB of HBM per device.

v0:
```python
import jax
import jax.numpy as jnp
from jax import lax
from jax.sharding import PartitionSpec as P

WINDOW = 128
EPS = 1e-06


def extended(x, sides, width):
    for axis, dim in sides:
        count, length = (lax.axis_size(axis), x.shape[dim])
        up = [(i, (i + 1) % count) for i in range(count - 1)]
        down = [(j, i) for i, j in up]
        last = lax.slice_in_dim(x, length - width, length, axis=dim)
        initial = lax.slice_in_dim(x, 0, width, axis=dim)
        before = lax.ppermute(last, axis, up)
        after = lax.ppermute(initial, axis, down)
        x = jnp.concatenate([before, x, after], axis=dim)
    return x


def rms_scale(field, gain):
    wide = field.astype(jnp.float32)
    return wide * lax.rsqrt(jnp.mean(wide * wide, axis=-1, keepdims=True) + EPS) * gain


def mixer_partial(normed, w_up, w_down):
    upward = jnp.dot(
        normed, lax.all_gather(w_up, "sp", axis=0, tiled=True), preferred_element_type=jnp.float32
    )
    active = jnp.square(jax.nn.relu(upward)).astype(jnp.bfloat16)
    return jnp.dot(
        active, lax.all_gather(w_down, "sp", axis=1, tiled=True), preferred_element_type=jnp.float32
    )


def shards(
    resid, queries, keys, values, documents, q_gain, k_gain, sink, w_out, n_gain, w_up, w_down
):
    rows = resid.shape[0]
    head_size = q_gain.shape[0]
    heads_here = sink.shape[0]
    kv_here = keys.shape[1] // head_size
    group = heads_here // kv_here
    qnorm = rms_scale(queries.reshape(rows, kv_here, group, head_size), q_gain).astype(jnp.bfloat16)
    knorm = rms_scale(keys.reshape(rows, kv_here, head_size), k_gain).astype(jnp.bfloat16)
    vheads = values.reshape(rows, kv_here, head_size)
    doc_here = documents.astype(jnp.bfloat16)
    near_keys, near_values, near_docs = (
        extended(knorm, (("sp", 0),), WINDOW),
        extended(vheads, (("sp", 0),), WINDOW),
        extended(doc_here, (("sp", 0),), WINDOW),
    )
    offset = lax.axis_index("sp") * rows
    total = rows * lax.axis_size("sp")
    query_pos = offset + jnp.arange(rows, dtype=jnp.int32)
    key_pos = offset - WINDOW + jnp.arange(rows + 2 * WINDOW, dtype=jnp.int32)
    distance = key_pos[None, :] - query_pos[:, None]
    allowed = (jnp.abs(distance) <= WINDOW) & (key_pos[None, :] >= 0) & (key_pos[None, :] < total)
    allowed = allowed & (near_docs[None, :] == doc_here[:, None])
    heads_all = heads_here * lax.axis_size("tp")
    first_head = (lax.axis_index("tp") * heads_here).astype(jnp.float32)
    slopes = jnp.exp2(
        -8.0 * (first_head + jnp.arange(heads_here, dtype=jnp.float32) + 1.0) / heads_all
    )
    slopes = slopes.reshape(kv_here, group)
    sink_f = sink.reshape(kv_here, group)
    scores = jnp.einsum(
        "rkgd,skd->kgrs", qnorm, near_keys, preferred_element_type=jnp.float32
    ) * head_size ** (-0.5)
    scores = scores - slopes[:, :, None, None] * jnp.abs(distance).astype(jnp.float32)[None, None]
    scores = jnp.where(allowed[None, None], scores, jnp.float32(-1e30))
    highest = jnp.maximum(jnp.max(scores, axis=-1), sink_f[:, :, None])
    weights = jnp.exp(scores - highest[..., None])
    denom = jnp.sum(weights, axis=-1) + jnp.exp(sink_f[:, :, None] - highest)
    summed = jnp.einsum(
        "kgrs,skd->rkgd",
        weights.astype(jnp.bfloat16),
        near_values,
        preferred_element_type=jnp.float32,
    )
    attended = (
        (summed / denom.transpose(2, 0, 1)[..., None])
        .astype(jnp.bfloat16)
        .reshape(rows, heads_here * head_size)
    )
    head_mix = lax.psum(
        jnp.dot(attended, w_out, preferred_element_type=jnp.float32).astype(jnp.bfloat16), "tp"
    ).astype(jnp.float32)
    middle = (resid.astype(jnp.float32) + head_mix).astype(jnp.bfloat16)
    normed = rms_scale(middle, n_gain).astype(jnp.bfloat16)
    partial_sum = mixer_partial(normed, w_up, w_down)
    unit_mix = lax.psum(partial_sum.astype(jnp.bfloat16), "tp").astype(jnp.float32)
    return (middle.astype(jnp.float32) + unit_mix).astype(jnp.bfloat16)


def solution(mesh):
    placed = (
        P("sp", None),
        P("sp", "tp"),
        P("sp", "tp"),
        P("sp", "tp"),
        P("sp"),
        P(),
        P(),
        P("tp"),
        P("tp", None),
        P(),
        P("sp", "tp"),
        P("tp", "sp"),
    )
    return jax.shard_map(
        shards, mesh=mesh, in_specs=placed, out_specs=P("sp", None), check_vma=False
    )
```

profile of v0, /device:TPU:0, one launch (start us, length us, event | category | flops | bytes accessed | tf_op | source)
XLA Modules:
  0.0 589.4 jit_solution(10305533719375993461)
XLA Ops:
  7.4 0.7 convert_element_type.69
  8.1 0.5 fusion.45
  8.6 5.4 collective-permute-start.2
  14.1 1.3 collective-permute-start.3
  15.4 1.1 copy.22
  16.5 0.8 multiply_convert_fusion.1
  17.3 0.7 fusion.44
  18.0 5.2 collective-permute-start.4
  23.1 1.3 collective-permute-start.5
  24.4 0.9 fusion.43
  25.4 5.2 collective-permute-start
  30.6 0.6 fusion.37
  31.2 1.5 copy.23
  33.0 0.6 add_rsqrt_fusion
  33.6 0.3 fusion.20
  34.1 0.7 max.24
  35.0 1.3 collective-permute-start.1
  36.3 0.7 pad_maximum_fusion
  37.0 1.8 fusion.24
  38.8 12.5 %fusion.3 = (f32[4,4,512]{2,1,0:T(4,128)S(1)}, f32[4,768,512,4]{2,1,3,0:T(8,128)}) fusion(f32[512,768]{0,1:T(8,128)S(1)} %fusion.20, f32[4,4]{1,0:T(4,128)S(1)} %multiply_exponential_fusion, pred[512,768]{0,1:T(8,128)(4,1)S(1)} %fusion.24, bf16[512,4,4,64]{0,3,2,1:T(8,128)(2,1)S(1)} %bitcast.50, f32[64]{0:T(128)} %param.17, f32[512,4,4]{0,2,1:T(4,128)} %add_rsqrt_fusion, ...), kind=kOutput, calls=%fused_computation.5 | convolution fusion | flops 840032256 | bytes 28639552 | tf_op jit(solution)/shard_map/rkgd,skd->kgrs/dot_general | solution.py:69
  51.3 12.1 %fusion.1 = f32[4,4,512]{2,1,0:T(4,128)S(1)} fusion(f32[4,768,512,4]{2,1,3,0:T(8,128)} %get-tuple-element.12, f32[4,4,512]{2,1,0:T(4,128)S(1)} %broadcast_maximum_fusion, f32[512,768]{0,1:T(8,128)S(1)} %fusion.20, f32[4,4]{1,0:T(4,128)S(1)} %multiply_exponential_fusion, pred[512,768]{0,1:T(8,128)(4,1)S(1)} %fusion.24), kind=kLoop, calls=%fused_computation.3 | loop fusion | flops 37740544 | bytes 27197504 | tf_op jit(solution)/shard_map/reduce_sum | solution.py:76
  63.5 12.5 %fusion.15 = bf16[512,4,4,64]{0,3,2,1:T(8,128)(2,1)S(1)} fusion(f32[4,768,512,4]{2,1,3,0:T(8,128)} %get-tuple-element.12, f32[4,4,512]{2,1,0:T(4,128)S(1)} %broadcast_maximum_fusion, f32[512,768]{0,1:T(8,128)S(1)} %fusion.20, f32[4,4]{1,0:T(4,128)S(1)} %multiply_exponential_fusion, pred[512,768]{0,1:T(8,128)(4,1)S(1)} %fusion.24, ...), kind=kOutput, calls=%fused_computation.25 | convolution fusion | flops 845283328 | bytes 28639296 | tf_op jit(solution)/shard_map/kgrs,skd->rkgd/dot_general | solution.py:77
  76.0 3.8 convolution_convert_fusion
  79.9 0.5 all-gather.3.cloned.1.call-update
  80.4 0.5 all-gather.5.cloned.1.call-update
  81.2 24.2 %all-reduce.3.cloned.1.call-done = bf16[512,2048]{1,0:T(8,128)(2,1)} async-done(((bf16[512,2048]{1,0:T(8,128)(2,1)}), bf16[512,2048]{1,0:T(8,128)(2,1)}) %all-reduce.3.cloned.1.call-update) | async-done | bytes 2097168 | tf_op jit(solution)/shard_map/psum | solution.py:88
  105.4 2.4 fusion.7
  107.8 170.2 %all-gather.3.cloned.1.call-done = bf16[2048,4096]{1,0:T(8,128)(2,1)} async-done(((bf16[128,4096]{1,0:T(8,128)(2,1)}), bf16[2048,4096]{1,0:T(8,128)(2,1)}) %all-gather.3.cloned.1.call-update) | async-done | bytes 16777232 | tf_op jit(solution)/shard_map/all_gather | solution.py:30
  278.0 249.7 %all-gather.5.cloned.1.call-done = bf16[4096,2048]{1,0:T(8,128)(2,1)} async-done(((bf16[4096,128]{1,0:T(8,128)(2,1)}), bf16[4096,2048]{1,0:T(8,128)(2,1)}) %all-gather.5.cloned.1.call-update) | async-done | bytes 16777232 | tf_op jit(solution)/shard_map/all_gather | solution.py:34
  527.7 29.8 %convolution_convert_fusion.1 = bf16[512,2048]{1,0:T(8,128)(2,1)} fusion(bf16[4096,2048]{1,0:T(8,128)(2,1)} %all-gather.5.cloned.1.call-done, bf16[2048,4096]{1,0:T(8,128)(2,1)} %all-gather.3.cloned.1.call-done, f32[2048]{0:T(1024)S(1)} %copy-done.3, f32[512]{0:T(512)S(1)} %add_rsqrt_fusion.2, bf16[512,2048]{1,0:T(8,128)(2,1)} %all-reduce.3.cloned.1.call-done, ...), kind=kOutput, calls=%fused_computation.18 | convolution fusion | flops 17195597824 | bytes 39856128 | tf_op jit(solution)/shard_map/dot_general | solution.py:33
  557.6 19.6 %all-reduce.5.cloned.1.call-done = bf16[512,2048]{1,0:T(8,128)(2,1)} async-done(((bf16[512,2048]{1,0:T(8,128)(2,1)}), bf16[512,2048]{1,0:T(8,128)(2,1)}) %all-reduce.5.cloned.1.call-update) | async-done | bytes 2097168 | tf_op jit(solution)/shard_map/psum | solution.py:94
  577.2 4.8 fusion.10
  (32 shorter events, 1.3 us)
Async XLA Ops:
  7.4 26.6 %copy-start.1 = (bf16[512,256]{1,0:T(8,128)(2,1)S(1)}, bf16[512,256]{1,0:T(8,128)(2,1)}, u32[]{:S(2)}) copy-start(bf16[512,256]{1,0:T(8,128)(2,1)} %param.15) | copy-start | bytes 786436
  7.4 98.0 %all-reduce.3.cloned.1.call-start = ((), (), s32[]{:S(2)}) async-start(), calls=%async_computation | async-start | bytes 4194304 | tf_op jit(solution)/shard_map/psum | solution.py:88
  8.6 26.3 %collective-permute-start.2 = (bf16[128]{0:T(256)(128)(2,1)}, bf16[128]{0:T(256)(128)(2,1)}, u32[]{:S(2)}, u32[]{:S(2)}) collective-permute-start(bf16[128]{0:T(256)(128)(2,1)} %get-tuple-element.9), channel_id=1, source_target_pairs={{0,2},{2,4},{4,6},{6,8},{8,10},{10,12},{12,14},{14,16},{16,18},{18... | collective-permute-start | bytes 776 | tf_op jit(solution)/shard_map/ppermute | solution.py:17
  14.1 22.2 %collective-permute-start.3 = (bf16[128]{0:T(256)(128)(2,1)}, bf16[128]{0:T(256)(128)(2,1)}, u32[]{:S(2)}, u32[]{:S(2)}) collective-permute-start(bf16[128]{0:T(256)(128)(2,1)} %get-tuple-element.10), channel_id=1, source_target_pairs={{2,0},{4,2},{6,4},{8,6},{10,8},{12,10},{14,12},{16,14},{18,16},{20... | collective-permute-start | bytes 776 | tf_op jit(solution)/shard_map/ppermute | solution.py:18
  18.0 20.8 %collective-permute-start.4 = (bf16[128,4,64]{0,2,1:T(8,128)(2,1)}, bf16[128,4,64]{0,2,1:T(8,128)(2,1)}, u32[]{:S(2)}, u32[]{:S(2)}) collective-permute-start(bf16[128,4,64]{0,2,1:T(8,128)(2,1)} %get-tuple-element.7), channel_id=1, source_target_pairs={{0,2},{2,4},{4,6},{6,8},{8,10},{10,12},{12,14},{14,16},{16,18},{18... | collective-permute-start | bytes 196616 | tf_op jit(solution)/shard_map/ppermute | solution.py:17
  23.1 15.6 %collective-permute-start.5 = (bf16[128,4,64]{0,2,1:T(8,128)(2,1)}, bf16[128,4,64]{0,2,1:T(8,128)(2,1)}, u32[]{:S(2)}, u32[]{:S(2)}) collective-permute-start(bf16[128,4,64]{0,2,1:T(8,128)(2,1)} %get-tuple-element.8), channel_id=1, source_target_pairs={{2,0},{4,2},{6,4},{8,6},{10,8},{12,10},{14,12},{16,14},{18,16},{20... | collective-permute-start | bytes 196616 | tf_op jit(solution)/shard_map/ppermute | solution.py:18
  25.4 38.0 %collective-permute-start = (bf16[128,4,64]{0,2,1:T(8,128)(2,1)S(1)}, bf16[128,4,64]{0,2,1:T(8,128)(2,1)}, u32[]{:S(2)}, u32[]{:S(2)}) collective-permute-start(bf16[128,4,64]{0,2,1:T(8,128)(2,1)S(1)} %bitcast.52), channel_id=1, source_target_pairs={{0,2},{2,4},{4,6},{6,8},{8,10},{10,12},{12,14},{14,16},{16,18},{18... | collective-permute-start | bytes 196616 | tf_op jit(solution)/shard_map/ppermute | solution.py:17
  35.0 28.5 %collective-permute-start.1 = (bf16[128,4,64]{0,2,1:T(8,128)(2,1)S(1)}, bf16[128,4,64]{0,2,1:T(8,128)(2,1)S(1)}, u32[]{:S(2)}, u32[]{:S(2)}) collective-permute-start(bf16[128,4,64]{0,2,1:T(8,128)(2,1)S(1)} %bitcast.53), channel_id=1, source_target_pairs={{2,0},{4,2},{6,4},{8,6},{10,8},{12,10},{14,12},{16,14},{18,16},{20... | collective-permute-start | bytes 196616 | tf_op jit(solution)/shard_map/ppermute | solution.py:18
  63.5 12.5 %copy-start.2 = (bf16[1024,2048]{1,0:T(8,128)(2,1)S(1)}, bf16[1024,2048]{1,0:T(8,128)(2,1)}, u32[]{:S(2)}) copy-start(bf16[1024,2048]{1,0:T(8,128)(2,1)} %param.20) | copy-start | bytes 12582916
  79.8 25.6 %copy-start = (bf16[512,2048]{1,0:T(8,128)(2,1)S(1)}, bf16[512,2048]{1,0:T(8,128)(2,1)}, u32[]{:S(2)}) copy-start(bf16[512,2048]{1,0:T(8,128)(2,1)} %param.12) | copy-start | bytes 6291460
  79.8 447.9 %copy-start.3 = (f32[2048]{0:T(1024)S(1)}, f32[2048]{0:T(1024)}, u32[]{:S(2)}) copy-start(f32[2048]{0:T(1024)} %param.21) | copy-start | bytes 24580
  79.8 198.2 %all-gather.3.cloned.1.call-start = ((), (), s32[]{:S(2)}) async-start(), calls=%async_computation.1 | async-start | bytes 17825792 | tf_op jit(solution)/shard_map/all_gather | solution.py:30
  80.4 447.3 %all-gather.5.cloned.1.call-start = ((), (), s32[]{:S(2)}) async-start(), calls=%async_computation.2 | async-start | bytes 17825792 | tf_op jit(solution)/shard_map/all_gather | solution.py:34
  81.0 496.2 %all-reduce.5.cloned.1.call-start = ((), (), s32[]{:S(2)}) async-start(), calls=%async_computation.3 | async-start | bytes 4194304 | tf_op jit(solution)/shard_map/psum | solution.py:94
Sparse Core Ops, SparseCore 0:
  79.9 25.4 all-reduce.2
  557.7 19.4 all-reduce.4
Sparse Core Ops, SparseCore 1:
  83.1 194.9 all-gather.2
  280.6 247.1 all-gather.4
where the time goes:
time: 590 us; the launch traced here: 589 us
  waiting for transfers between devices  465 us (79%)
  matrix products  58.5 us (10%)
  other arithmetic  25.2 us (4%)
  starting transfers between devices  19.9 us (3%)
  between operations  15 us (3%)
    all_gather x1, waiting for transfers between devices, mixer_partial(): lax.all_gather(w_down, 'sp', axis=1, tiled=True)  250 us
    all_gather x1, waiting for transfers between devices, mixer_partial(): lax.all_gather(w_up, 'sp', axis=0, tiled=True)  170 us
    dot_general x1, matrix products, mixer_partial(): jnp.dot(active, lax.all_gather(w_down, 'sp', axis=1, tiled=True), preferr...  29.8 us
    psum x1, waiting for transfers between devices, shards(): lax.psum(jnp.dot(attended, w_out, preferred_element_type=jnp.float32).ast...  24.2 us
    psum x1, waiting for transfers between devices, shards(): lax.psum(partial_sum.astype(jnp.bfloat16), 'tp').astype(jnp.float32)  19.6 us
    ppermute x3, starting transfers between devices, extended(): before = lax.ppermute(last, axis, up)  15.8 us
    dot_general x1, matrix products, shards(): jnp.einsum('kgrs,skd->rkgd', weights.astype(jnp.bfloat16), near_values, p...  12.5 us
    dot_general x1, matrix products, shards(): jnp.einsum('rkgd,skd->kgrs', qnorm, near_keys, preferred_element_type=jnp...  12.5 us
  transfers between devices with their start and end apart: 10, of which 4 were waited for; matrix products, arithmetic and copies ran while one was open for 6% of the time, Pallas kernels for 0%

commit v1 on v0

--- a/solution.py
+++ b/solution.py
@@ -5,6 +5,12 @@
 
 WINDOW = 128
 EPS = 1e-06
+
+
+def all_parts(x, name, along):
+    shards = lax.all_gather(x, name, axis=0, tiled=False)
+    whole = jnp.concatenate(shards, axis=along)
+    return whole
 
 
 def extended(x, sides, width):
@@ -30,9 +36,7 @@
         normed, lax.all_gather(w_up, "sp", axis=0, tiled=True), preferred_element_type=jnp.float32
     )
     active = jnp.square(jax.nn.relu(upward)).astype(jnp.bfloat16)
-    return jnp.dot(
-        active, lax.all_gather(w_down, "sp", axis=1, tiled=True), preferred_element_type=jnp.float32
-    )
+    return jnp.dot(active, all_parts(w_down, "sp", 1), preferred_element_type=jnp.float32)
 
 
 def shards(

time: 590 us -> 527 us (0.89)
  waiting for transfers between devices: 465 us -> 385 us
  local copies, waits for them, and re-layouts: 5.81 us -> 27.1 us
    all_gather x1, waiting for transfers between devices: 250 us -> 170 us  [all_parts(): shards = lax.all_gather(x, name, axis=0, tiled=False)]
    reshape x0 -> x1, local copies, waits for them, and re-layouts: none -> 21.3 us  [all_parts(): whole = jnp.concatenate(shards, axis=along)]
  transfers between devices with their start and end apart: 10 -> 10, of which waited for: 4 -> 4; matrix products, arithmetic and copies ran while one was open for 6% -> 11% of each run, Pallas kernels for 0% -> 0%
where the time goes in v1:
time: 527 us; the launch traced here: 525 us
  waiting for transfers between devices  385 us (73%)
  matrix products  52.7 us (10%)
  local copies, waits for them, and re-layouts  27.1 us (5%)
  other arithmetic  25.2 us (5%)
  starting transfers between devices  19.9 us (4%)
  between operations  15 us (3%)
    all_gather x1, waiting for transfers between devices, mixer_partial(): lax.all_gather(w_up, 'sp', axis=0, tiled=True)  170 us
    all_gather x1, waiting for transfers between devices, all_parts(): shards = lax.all_gather(x, name, axis=0, tiled=False)  170 us
    psum x1, waiting for transfers between devices, shards(): lax.psum(jnp.dot(attended, w_out, preferred_element_type=jnp.float32).ast...  24.2 us
    dot_general x1, matrix products, mixer_partial(): jnp.dot(active, all_parts(w_down, 'sp', 1), preferred_element_type=jnp.fl...  24 us
    reshape x1, local copies, waits for them, and re-layouts, all_parts(): whole = jnp.concatenate(shards, axis=along)  21.3 us
    psum x1, waiting for transfers between devices, shards(): lax.psum(partial_sum.astype(jnp.bfloat16), 'tp').astype(jnp.float32)  19.6 us
    ppermute x3, starting transfers between devices, extended(): before = lax.ppermute(last, axis, up)  15.8 us
    dot_general x1, matrix products, shards(): jnp.einsum('kgrs,skd->rkgd', weights.astype(jnp.bfloat16), near_values, p...  12.5 us
  transfers between devices with their start and end apart: 10, of which 4 were waited for; matrix products, arithmetic and copies ran while one was open for 11% of the time, Pallas kernels for 0%

profile of v1, /device:TPU:0, one launch (start us, length us, event | category | flops | bytes accessed | tf_op | source)
XLA Modules:
  0.0 525.4 jit_solution(11413519610624904754)
XLA Ops:
  7.4 0.7 convert_element_type.69
  8.1 0.5 fusion.50
  8.6 5.4 %collective-permute-start.2 = (bf16[128]{0:T(256)(128)(2,1)}, bf16[128]{0:T(256)(128)(2,1)}, u32[]{:S(2)}, u32[]{:S(2)}) collective-permute-start(bf16[128]{0:T(256)(128)(2,1)} %get-tuple-element.9), channel_id=1, source_target_pairs={{0,2},{2,4},{4,6},{6,8},{8,10},{10,12},{12,14},{14,16},{16,18},{18... | collective-permute-start | bytes 776 | tf_op jit(solution)/shard_map/ppermute | solution.py:23
  14.1 1.3 collective-permute-start.3
  15.4 1.1 copy.28
  16.5 0.8 multiply_convert_fusion.1
  17.3 0.7 fusion.49
  18.0 5.2 collective-permute-start.4
  23.1 1.3 collective-permute-start.5
  24.4 0.9 fusion.48
  25.4 5.2 collective-permute-start
  30.6 0.6 fusion.41
  31.2 1.5 copy.29
  33.0 0.6 add_rsqrt_fusion
  34.1 0.7 max.24
  35.0 1.3 collective-permute-start.1
  36.3 0.7 pad_maximum_fusion
  37.0 1.8 fusion.28
  38.8 12.5 %fusion.3 = (f32[4,4,512]{2,1,0:T(4,128)S(1)}, f32[4,768,512,4]{2,1,3,0:T(8,128)}) fusion(f32[512,768]{0,1:T(8,128)S(1)} %fusion.24, f32[4,4]{1,0:T(4,128)S(1)} %multiply_exponential_fusion, pred[512,768]{0,1:T(8,128)(4,1)S(1)} %fusion.28, bf16[512,4,4,64]{0,3,2,1:T(8,128)(2,1)S(1)} %bitcast.51, f32[64]{0:T(128)} %param.17, f32[512,4,4]{0,2,1:T(4,128)} %add_rsqrt_fusion, ...), kind=kOutput, calls=%fused_computation.5 | convolution fusion | flops 840032256 | bytes 28639552 | tf_op jit(solution)/shard_map/rkgd,skd->kgrs/dot_general | solution.py:73
  51.3 12.1 %fusion.1 = f32[4,4,512]{2,1,0:T(4,128)S(1)} fusion(f32[4,768,512,4]{2,1,3,0:T(8,128)} %get-tuple-element.12, f32[4,4,512]{2,1,0:T(4,128)S(1)} %broadcast_maximum_fusion, f32[512,768]{0,1:T(8,128)S(1)} %fusion.24, f32[4,4]{1,0:T(4,128)S(1)} %multiply_exponential_fusion, pred[512,768]{0,1:T(8,128)(4,1)S(1)} %fusion.28), kind=kLoop, calls=%fused_computation.3 | loop fusion | flops 37740544 | bytes 27197504 | tf_op jit(solution)/shard_map/reduce_sum | solution.py:80
  63.5 12.5 %fusion.17 = bf16[512,4,4,64]{0,3,2,1:T(8,128)(2,1)S(1)} fusion(f32[4,768,512,4]{2,1,3,0:T(8,128)} %get-tuple-element.12, f32[4,4,512]{2,1,0:T(4,128)S(1)} %broadcast_maximum_fusion, f32[512,768]{0,1:T(8,128)S(1)} %fusion.24, f32[4,4]{1,0:T(4,128)S(1)} %multiply_exponential_fusion, pred[512,768]{0,1:T(8,128)(4,1)S(1)} %fusion.28, ...), kind=kOutput, calls=%fused_computation.25 | convolution fusion | flops 845283328 | bytes 28639296 | tf_op jit(solution)/shard_map/kgrs,skd->rkgd/dot_general | solution.py:81
  76.0 3.8 convolution_convert_fusion
  79.8 0.5 all-gather.6.cloned.1.call-update
  80.4 0.5 all-gather.4.cloned.1.call-update
  81.2 24.2 %all-reduce.3.cloned.1.call-done = bf16[512,2048]{1,0:T(8,128)(2,1)} async-done(((bf16[512,2048]{1,0:T(8,128)(2,1)}), bf16[512,2048]{1,0:T(8,128)(2,1)}) %all-reduce.3.cloned.1.call-update) | async-done | bytes 2097168 | tf_op jit(solution)/shard_map/psum | solution.py:92
  105.4 2.4 fusion.7
  107.8 170.2 %all-gather.6.cloned.1.call-done = bf16[65536,128]{1,0:T(8,128)(2,1)} async-done(((bf16[4096,128]{1,0:T(8,128)(2,1)}), bf16[65536,128]{1,0:T(8,128)(2,1)}) %all-gather.6.cloned.1.call-update) | async-done | bytes 16777232 | tf_op jit(solution)/shard_map/all_gather | solution.py:11
  278.0 21.3 %copy.31 = bf16[4096,16,128]{0,2,1:T(8,128)(2,1)} copy(bf16[4096,16,128]{2,0,1:T(8,128)(2,1)} %bitcast.49) | data formatting | bytes 33554432 | tf_op jit(solution)/shard_map/reshape | solution.py:12
  299.3 170.3 %all-gather.4.cloned.1.call-done = bf16[2048,4096]{1,0:T(8,128)(2,1)} async-done(((bf16[128,4096]{1,0:T(8,128)(2,1)}), bf16[2048,4096]{1,0:T(8,128)(2,1)}) %all-gather.4.cloned.1.call-update) | async-done | bytes 16777232 | tf_op jit(solution)/shard_map/all_gather | solution.py:36
  469.6 24.0 %convolution_convert_fusion.1 = bf16[512,2048]{1,0:T(8,128)(2,1)} fusion(bf16[4096,2048]{0,1:T(8,128)(2,1)} %bitcast.50, bf16[2048,4096]{1,0:T(8,128)(2,1)} %all-gather.4.cloned.1.call-done, f32[2048]{0:T(1024)S(1)} %copy-done.3, f32[512]{0:T(512)S(1)} %add_rsqrt_fusion.2, bf16[512,2048]{1,0:T(8,128)(2,1)} %all-reduce.3.cloned.1.call-done, ...), kind=kOutput, calls=%fused_computation.18 | convolution fusion | flops 17195597824 | bytes 39856128 | tf_op jit(solution)/shard_map/dot_general | solution.py:39
  493.6 19.6 %all-reduce.5.cloned.1.call-done = bf16[512,2048]{1,0:T(8,128)(2,1)} async-done(((bf16[512,2048]{1,0:T(8,128)(2,1)}), bf16[512,2048]{1,0:T(8,128)(2,1)}) %all-reduce.5.cloned.1.call-update) | async-done | bytes 2097168 | tf_op jit(solution)/shard_map/psum | solution.py:98
  513.2 4.8 fusion.10
  (33 shorter events, 1.6 us)
Async XLA Ops:
  7.4 26.6 %copy-start.1 = (bf16[512,256]{1,0:T(8,128)(2,1)S(1)}, bf16[512,256]{1,0:T(8,128)(2,1)}, u32[]{:S(2)}) copy-start(bf16[512,256]{1,0:T(8,128)(2,1)} %param.15) | copy-start | bytes 786436
  7.4 98.0 %all-reduce.3.cloned.1.call-start = ((), (), s32[]{:S(2)}) async-start(), calls=%async_computation | async-start | bytes 4194304 | tf_op jit(solution)/shard_map/psum | solution.py:92
  8.6 26.3 %collective-permute-start.2 = (bf16[128]{0:T(256)(128)(2,1)}, bf16[128]{0:T(256)(128)(2,1)}, u32[]{:S(2)}, u32[]{:S(2)}) collective-permute-start(bf16[128]{0:T(256)(128)(2,1)} %get-tuple-element.9), channel_id=1, source_target_pairs={{0,2},{2,4},{4,6},{6,8},{8,10},{10,12},{12,14},{14,16},{16,18},{18... | collective-permute-start | bytes 776 | tf_op jit(solution)/shard_map/ppermute | solution.py:23
  14.1 22.2 %collective-permute-start.3 = (bf16[128]{0:T(256)(128)(2,1)}, bf16[128]{0:T(256)(128)(2,1)}, u32[]{:S(2)}, u32[]{:S(2)}) collective-permute-start(bf16[128]{0:T(256)(128)(2,1)} %get-tuple-element.10), channel_id=1, source_target_pairs={{2,0},{4,2},{6,4},{8,6},{10,8},{12,10},{14,12},{16,14},{18,16},{20... | collective-permute-start | bytes 776 | tf_op jit(solution)/shard_map/ppermute | solution.py:24
  18.0 20.8 %collective-permute-start.4 = (bf16[128,4,64]{0,2,1:T(8,128)(2,1)}, bf16[128,4,64]{0,2,1:T(8,128)(2,1)}, u32[]{:S(2)}, u32[]{:S(2)}) collective-permute-start(bf16[128,4,64]{0,2,1:T(8,128)(2,1)} %get-tuple-element.7), channel_id=1, source_target_pairs={{0,2},{2,4},{4,6},{6,8},{8,10},{10,12},{12,14},{14,16},{16,18},{18... | collective-permute-start | bytes 196616 | tf_op jit(solution)/shard_map/ppermute | solution.py:23
  23.1 15.6 %collective-permute-start.5 = (bf16[128,4,64]{0,2,1:T(8,128)(2,1)}, bf16[128,4,64]{0,2,1:T(8,128)(2,1)}, u32[]{:S(2)}, u32[]{:S(2)}) collective-permute-start(bf16[128,4,64]{0,2,1:T(8,128)(2,1)} %get-tuple-element.8), channel_id=1, source_target_pairs={{2,0},{4,2},{6,4},{8,6},{10,8},{12,10},{14,12},{16,14},{18,16},{20... | collective-permute-start | bytes 196616 | tf_op jit(solution)/shard_map/ppermute | solution.py:24
  25.4 38.0 %collective-permute-start = (bf16[128,4,64]{0,2,1:T(8,128)(2,1)S(1)}, bf16[128,4,64]{0,2,1:T(8,128)(2,1)}, u32[]{:S(2)}, u32[]{:S(2)}) collective-permute-start(bf16[128,4,64]{0,2,1:T(8,128)(2,1)S(1)} %bitcast.53), channel_id=1, source_target_pairs={{0,2},{2,4},{4,6},{6,8},{8,10},{10,12},{12,14},{14,16},{16,18},{18... | collective-permute-start | bytes 196616 | tf_op jit(solution)/shard_map/ppermute | solution.py:23
  35.0 28.5 %collective-permute-start.1 = (bf16[128,4,64]{0,2,1:T(8,128)(2,1)S(1)}, bf16[128,4,64]{0,2,1:T(8,128)(2,1)S(1)}, u32[]{:S(2)}, u32[]{:S(2)}) collective-permute-start(bf16[128,4,64]{0,2,1:T(8,128)(2,1)S(1)} %bitcast.54), channel_id=1, source_target_pairs={{2,0},{4,2},{6,4},{8,6},{10,8},{12,10},{14,12},{16,14},{18,16},{20... | collective-permute-start | bytes 196616 | tf_op jit(solution)/shard_map/ppermute | solution.py:24
  63.5 12.5 %copy-start.2 = (bf16[1024,2048]{1,0:T(8,128)(2,1)S(1)}, bf16[1024,2048]{1,0:T(8,128)(2,1)}, u32[]{:S(2)}) copy-start(bf16[1024,2048]{1,0:T(8,128)(2,1)} %param.20) | copy-start | bytes 12582916
  79.8 25.6 %copy-start = (bf16[512,2048]{1,0:T(8,128)(2,1)S(1)}, bf16[512,2048]{1,0:T(8,128)(2,1)}, u32[]{:S(2)}) copy-start(bf16[512,2048]{1,0:T(8,128)(2,1)} %param.12) | copy-start | bytes 6291460
  79.8 198.2 %all-gather.6.cloned.1.call-start = ((), (), s32[]{:S(2)}) async-start(), calls=%async_computation.3 | async-start | bytes 17825792 | tf_op jit(solution)/shard_map/all_gather | solution.py:11
  80.4 389.2 %all-gather.4.cloned.1.call-start = ((), (), s32[]{:S(2)}) async-start(), calls=%async_computation.1 | async-start | bytes 17825792 | tf_op jit(solution)/shard_map/all_gather | solution.py:36
  81.0 432.3 %all-reduce.5.cloned.1.call-start = ((), (), s32[]{:S(2)}) async-start(), calls=%async_computation.2 | async-start | bytes 4194304 | tf_op jit(solution)/shard_map/psum | solution.py:98
  278.0 191.6 %copy-start.3 = (f32[2048]{0:T(1024)S(1)}, f32[2048]{0:T(1024)}, u32[]{:S(2)}) copy-start(f32[2048]{0:T(1024)} %param.21) | copy-start | bytes 24580
Sparse Core Ops, SparseCore 0:
  79.9 25.4 all-reduce.2
  493.7 19.4 all-reduce.4
Sparse Core Ops, SparseCore 1:
  83.0 194.9 all-gather.5
  280.6 188.9 all-gather.3
